TPU v7x, 32 devices: a whole 2x2x4 slice. The times are simulated.
32 devices in a mesh: sp: 4 (over y, x), tp: 8 (over z, core).
Axes of the slice: x: 2, y: 2, z: 4, core: 2. Of those that a mesh axis runs over, the one named last changes fastest.
Arguments:
- tokens: bfloat16 [2048, 4096], P('sp', 'tp'), may hold values from -6 to 6
- pre_gain: float32 [2, 4096], replicated, may hold values from 0.1 to 1.9
- w_value: bfloat16 [2, 4096, 4096], P(None, 'sp', 'tp'), may hold values from -0.09375 to 0.09375
- w_gate: bfloat16 [2, 4096, 4096], P(None, 'sp', 'tp'), may hold values from -0.09375 to 0.09375
- conv_taps: float32 [2, 31, 4096], P(None, None, 'tp'), may hold values from -3.5 to 3.5
- conv_bias: float32 [2, 4096], P(None, 'tp'), may hold values from -3 to 3
- norm_gain: float32 [2, 4096], P(None, 'tp'), may hold values from 0.1 to 1.9
- norm_bias: float32 [2, 4096], P(None, 'tp'), may hold values from -3 to 3
- w_out: bfloat16 [2, 4096, 4096], P(None, 'sp', 'tp'), may hold values from -0.09375 to 0.09375
- post_gain: float32 [2, 4096], P(None, 'tp'), may hold values from 0.1 to 1.9
Outputs:
- stream: bfloat16 [2048, 4096], P('sp', 'tp')
All inputs are finite; a program needn't handle non-finite values.
Results may differ from a plain program's by a relative error of at most 0.009.
Values may be sent and summed in bfloat16 or wider, within the bound.
A program may use at most 64 MiB of HBM per device.

v0:
```python
import jax
import jax.numpy as jnp
from jax import lax
from jax.sharding import PartitionSpec as P


def passed_along(value, axis, steps):
    count = lax.axis_size(axis)
    leading, last = (max(0, -steps), min(count, count - steps))
    return lax.ppermute(value, axis, [(source, source + steps) for source in range(leading, last)])


def shards(
    tokens, pre_gain, w_value, w_gate, conv_taps, conv_bias, norm_gain, norm_bias, w_out, post_gain
):
    layer_count = w_value.shape[0]
    tap_count = conv_taps.shape[1]
    channel_count = conv_taps.shape[2] * lax.axis_size("tp")
    model_width = tokens.shape[1] * lax.axis_size("tp")
    local_rows = tokens.shape[0]
    every_value, every_gate, every_out = (
        lax.all_gather(w_value, "sp", axis=1, tiled=True),
        lax.all_gather(w_gate, "sp", axis=1, tiled=True),
        lax.all_gather(w_out, "sp", axis=1, tiled=True),
    )
    stream = tokens
    for layer_index in range(layer_count):
        gathered = lax.all_gather(stream, "tp", axis=1, tiled=True)
        full_rows = gathered.astype(jnp.float32)
        scale_rows = lax.rsqrt(jnp.mean(full_rows * full_rows, axis=-1, keepdims=True) + 1e-06)
        normed = (full_rows * scale_rows * pre_gain[layer_index]).astype(jnp.bfloat16)
        value_block = every_value[layer_index]
        gate_block = every_gate[layer_index]
        out_block = every_out[layer_index]
        value_proj = jnp.dot(normed, value_block, preferred_element_type=jnp.float32)
        gate_proj = jnp.dot(normed, gate_block, preferred_element_type=jnp.float32)
        glu_out = (value_proj * jax.nn.sigmoid(gate_proj)).astype(jnp.bfloat16)
        earlier = passed_along(glu_out[local_rows - (tap_count - 1) :], "sp", 1)
        padded = jnp.concatenate([earlier, glu_out], axis=0).astype(jnp.float32)
        filtered = jnp.zeros(glu_out.shape, jnp.float32) + conv_bias[layer_index]
        for tap_index in range(tap_count):
            filtered = (
                filtered
                + padded[tap_index : tap_index + local_rows] * conv_taps[layer_index, tap_index]
            )
        channel_sum, channel_square = lax.psum(
            (jnp.sum(filtered, axis=-1), jnp.sum(filtered * filtered, axis=-1)), "tp"
        )
        centre = channel_sum / channel_count
        spread = jnp.maximum(channel_square / channel_count - centre * centre, 0.0)
        shaped = (filtered - centre[:, None]) * lax.rsqrt(spread + 1e-05)[:, None]
        mixed = jax.nn.silu(shaped * norm_gain[layer_index] + norm_bias[layer_index]).astype(
            jnp.bfloat16
        )
        whole_mixed = lax.all_gather(mixed, "tp", axis=1, tiled=True)
        branch_low = jnp.dot(whole_mixed, out_block, preferred_element_type=jnp.float32).astype(
            jnp.bfloat16
        )
        branch = lax.optimization_barrier(branch_low).astype(jnp.float32)
        total = lax.psum(jnp.sum(branch * branch, axis=-1), "tp")
        rescale = lax.rsqrt(total / model_width + 1e-06)[:, None]
        stream = (stream.astype(jnp.float32) + branch * rescale * post_gain[layer_index]).astype(
            jnp.bfloat16
        )
    return stream


def solution(mesh):
    in_specs = (
        P("sp", "tp"),
        P(),
        P(None, "sp", "tp"),
        P(None, "sp", "tp"),
        P(None, None, "tp"),
        P(None, "tp"),
        P(None, "tp"),
        P(None, "tp"),
        P(None, "sp", "tp"),
        P(None, "tp"),
    )
    out_specs = P("sp", "tp")
    return jax.shard_map(shards, mesh=mesh, in_specs=in_specs, out_specs=out_specs, check_vma=False)
```

profile of v0, /device:TPU:0, one launch (start us, length us, event | category | flops | bytes accessed | tf_op | source)
XLA Modules:
  0.0 551.2 jit_solution(2232420375245703278)
XLA Ops:
  6.5 0.0 all-gather.8.cloned.1.call-start
  6.6 0.7 all-gather.8.cloned.1.call-update
  7.3 0.0 all-gather.12.cloned.1.call-start
  7.3 0.7 all-gather.12.cloned.1.call-update
  8.0 0.0 all-gather.10.cloned.1.call-start
  8.1 0.7 all-gather.10.cloned.1.call-update
  8.8 0.0 all-gather.16.cloned.1.call-start
  8.8 0.5 all-gather.16.cloned.1.call-update
  9.3 0.0 all-gather.14.cloned.1.call-start
  9.6 49.0 %all-gather.8.cloned.1.call-done = bf16[512,4096]{1,0:T(8,128)(2,1)} async-done(((bf16[512,512]{1,0:T(8,128)(2,1)}), bf16[512,4096]{1,0:T(8,128)(2,1)}) %all-gather.8.cloned.1.call-update) | async-done | bytes 4194320 | tf_op jit(solution)/shard_map/all_gather | solution.py:28
  58.6 3.1 fusion
  61.7 85.1 %all-gather.12.cloned.1.call-done = bf16[2,4096,512]{2,1,0:T(8,128)(2,1)} async-done(((bf16[2,1024,512]{2,1,0:T(8,128)(2,1)}), bf16[2,4096,512]{2,1,0:T(8,128)(2,1)}) %all-gather.12.cloned.1.call-update) | async-done | bytes 8388624 | tf_op jit(solution)/shard_map/all_gather | solution.py:23
  146.7 6.0 %fusion.21 = f32[512,512]{1,0:T(8,128)S(1)} fusion(bf16[2,4096,512]{2,1,0:T(8,128)(2,1)} %all-gather.12.cloned.1.call-done, bf16[512,4096]{1,0:T(8,128)(2,1)} %all-gather.8.cloned.1.call-done, f32[4096]{0:T(1024)S(1)} %bitcast.122, f32[512]{0:T(512)S(1)} %add_rsqrt_fusion.5), kind=kOutput, calls=%fused_computation.35 | convolution fusion | flops 2156658688 | bytes 9455616 | tf_op jit(solution)/shard_map/dot_general | solution.py:36
  152.7 83.4 %all-gather.10.cloned.1.call-done = bf16[2,4096,512]{2,1,0:T(8,128)(2,1)} async-done(((bf16[2,1024,512]{2,1,0:T(8,128)(2,1)}), bf16[2,4096,512]{2,1,0:T(8,128)(2,1)}) %all-gather.10.cloned.1.call-update) | async-done | bytes 8388624 | tf_op jit(solution)/shard_map/all_gather | solution.py:22
  236.1 5.8 %fusion.23 = bf16[512,512]{1,0:T(8,128)(2,1)S(1)} fusion(f32[512,512]{1,0:T(8,128)S(1)} %fusion.21, bf16[2,4096,512]{2,1,0:T(8,128)(2,1)} %all-gather.10.cloned.1.call-done, bf16[512,4096]{1,0:T(8,128)(2,1)} %all-gather.8.cloned.1.call-done, f32[4096]{0:T(1024)S(1)} %bitcast.123, f32[512]{0:T(512)S(1)} %add_rsqrt_fusion.5), kind=kOutput, calls=%fused_computation.37 | convolution fusion | flops 2156396544 | bytes 9979904 | tf_op jit(solution)/shard_map/dot_general | solution.py:35
  242.0 3.4 collective-permute-start
  245.4 1.6 collective-permute-done
  246.9 0.2 maximum_convert_fusion
  247.1 5.0 fusion.101
  252.1 15.3 %all-reduce.1 = (f32[512]{0:T(512)S(1)}, f32[512]{0:T(512)S(1)}) all-reduce(f32[512]{0:T(512)S(1)} %get-tuple-element.8, f32[512]{0:T(512)S(1)} %get-tuple-element.7), channel_id=1, replica_groups=mesh['sp'=4,'tp'=8] {'tp'}, use_global_device_ids=true, to_apply=%region_4.0 | all-reduce | flops 1024 | bytes 8192 | tf_op jit(solution)/shard_map/psum | solution.py:46
  267.4 1.2 multiply_convert_fusion.1
  268.7 0.0 all-gather.14.cloned.1.call-update
  268.7 0.0 all-gather.18.cloned.1.call-start
  268.8 56.5 %all-gather.16.cloned.1.call-done = bf16[2,4096,512]{2,1,0:T(8,128)(2,1)} async-done(((bf16[2,1024,512]{2,1,0:T(8,128)(2,1)}), bf16[2,4096,512]{2,1,0:T(8,128)(2,1)}) %all-gather.16.cloned.1.call-update) | async-done | bytes 8388624 | tf_op jit(solution)/shard_map/all_gather | solution.py:24
  325.3 48.4 %all-gather.14.cloned.1.call-done = bf16[512,4096]{1,0:T(8,128)(2,1)} async-done(((bf16[512,512]{1,0:T(8,128)(2,1)}), bf16[512,4096]{1,0:T(8,128)(2,1)}) %all-gather.14.cloned.1.call-update) | async-done | bytes 4194320 | tf_op jit(solution)/shard_map/all_gather | solution.py:55
  373.7 5.8 %fusion.24 = bf16[512,512]{1,0:T(8,128)(2,1)S(1)} fusion(bf16[512,4096]{1,0:T(8,128)(2,1)} %all-gather.14.cloned.1.call-done, bf16[2,4096,512]{2,1,0:T(8,128)(2,1)} %all-gather.16.cloned.1.call-done), kind=kOutput, calls=%fused_computation.38 | convolution fusion | flops 2147745792 | bytes 8912896 | tf_op jit(solution)/shard_map/dot_general | solution.py:56
  379.5 0.2 fusion.30
  379.6 14.8 %psum.44 = f32[512]{0:T(512)S(1)} all-reduce(f32[512]{0:T(512)S(1)} %fusion.30), channel_id=1, replica_groups=mesh['sp'=4,'tp'=8] {'tp'}, use_global_device_ids=true, to_apply=%region_6.7 | all-reduce | flops 512 | bytes 4096 | tf_op jit(solution)/shard_map/psum | solution.py:60
  394.5 1.1 fusion.33
  395.5 0.0 all-gather.18.cloned.1.call-update
  395.5 0.2 all-gather.20.cloned.1.call-start
  395.8 44.7 %all-gather.18.cloned.1.call-done = bf16[512,4096]{1,0:T(8,128)(2,1)} async-done(((bf16[512,512]{1,0:T(8,128)(2,1)}), bf16[512,4096]{1,0:T(8,128)(2,1)}) %all-gather.18.cloned.1.call-update) | async-done | bytes 4194320 | tf_op jit(solution)/shard_map/all_gather | solution.py:28
  440.5 3.2 fusion.3
  443.7 0.2 copy-done.1
  443.9 5.0 fusion.19
  449.0 2.4 fusion.22
  451.4 3.4 collective-permute-start.1
  454.9 1.5 collective-permute-done.1
  456.4 0.2 maximum_convert_fusion.1
  456.5 5.0 fusion.100
  461.6 13.7 %all-reduce = (f32[512]{0:T(512)S(1)}, f32[512]{0:T(512)S(1)}) all-reduce(f32[512]{0:T(512)S(1)} %get-tuple-element.6, f32[512]{0:T(512)S(1)} %get-tuple-element.5), channel_id=1, replica_groups=mesh['sp'=4,'tp'=8] {'tp'}, use_global_device_ids=true, to_apply=%region_11.12 | all-reduce | flops 1024 | bytes 8192 | tf_op jit(solution)/shard_map/psum | solution.py:46
  475.3 1.3 multiply_convert_fusion
  476.6 0.0 all-gather.20.cloned.1.call-update
  476.6 45.9 %all-gather.20.cloned.1.call-done = bf16[512,4096]{1,0:T(8,128)(2,1)} async-done(((bf16[512,512]{1,0:T(8,128)(2,1)}), bf16[512,4096]{1,0:T(8,128)(2,1)}) %all-gather.20.cloned.1.call-update) | async-done | bytes 4194320 | tf_op jit(solution)/shard_map/all_gather | solution.py:55
  522.5 5.8 %fusion.25 = bf16[512,512]{1,0:T(8,128)(2,1)S(1)} fusion(bf16[512,4096]{1,0:T(8,128)(2,1)} %all-gather.20.cloned.1.call-done, bf16[2,4096,512]{2,1,0:T(8,128)(2,1)} %all-gather.16.cloned.1.call-done), kind=kOutput, calls=%fused_computation.39 | convolution fusion | flops 2147745792 | bytes 8912896 | tf_op jit(solution)/shard_map/dot_general | solution.py:56
  528.3 0.2 fusion.34
  528.5 14.8 %psum.47 = f32[512]{0:T(512)S(1)} all-reduce(f32[512]{0:T(512)S(1)} %fusion.34), channel_id=1, replica_groups=mesh['sp'=4,'tp'=8] {'tp'}, use_global_device_ids=true, to_apply=%region_13.14 | all-reduce | flops 512 | bytes 4096 | tf_op jit(solution)/shard_map/psum | solution.py:60
  543.3 1.1 fusion.37
  (39 shorter events, 0.3 us)
Async XLA Ops:
  6.5 2.8 copy-start.5
  6.5 2.9 copy-start.6
  6.5 2.9 copy-start.3
  6.5 3.0 copy-start.4
  6.5 52.0 %all-gather.8.cloned.1.call-start = ((), (), s32[]{:S(2)}) async-start(), calls=%async_computation | async-start | bytes 4718592 | tf_op jit(solution)/shard_map/all_gather | solution.py:28
  7.3 139.5 %all-gather.12.cloned.1.call-start = ((), (), s32[]{:S(2)}) async-start(), calls=%async_computation.2 | async-start | bytes 10485760 | tf_op jit(solution)/shard_map/all_gather | solution.py:23
  8.0 228.1 %all-gather.10.cloned.1.call-start = ((), (), s32[]{:S(2)}) async-start(), calls=%async_computation.1 | async-start | bytes 10485760 | tf_op jit(solution)/shard_map/all_gather | solution.py:22
  8.8 316.6 %all-gather.16.cloned.1.call-start = ((), (), s32[]{:S(2)}) async-start(), calls=%async_computation.4 | async-start | bytes 10485760 | tf_op jit(solution)/shard_map/all_gather | solution.py:24
  9.3 364.3 %all-gather.14.cloned.1.call-start = ((), (), s32[]{:S(2)}) async-start(), calls=%async_computation.3 | async-start | bytes 4718592 | tf_op jit(solution)/shard_map/all_gather | solution.py:55
  152.7 92.6 %copy-start.7 = (f32[2,512]{1,0:T(2,128)S(1)}, f32[2,512]{1,0:T(2,128)}, u32[]{:S(2)}) copy-start(f32[2,512]{1,0:T(2,128)} %param.16) | copy-start | bytes 12292
  242.0 5.0 collective-permute-start
  247.1 21.7 %copy-start.8 = (f32[2,512]{1,0:T(2,128)S(1)}, f32[2,512]{1,0:T(2,128)}, u32[]{:S(2)}) copy-start(f32[2,512]{1,0:T(2,128)} %param.19) | copy-start | bytes 12292
  268.7 171.8 %all-gather.18.cloned.1.call-start = ((), (), s32[]{:S(2)}) async-start(), calls=%async_computation.5 | async-start | bytes 4718592 | tf_op jit(solution)/shard_map/all_gather | solution.py:28
  268.8 125.7 %copy-start.2 = (bf16[512,512]{1,0:T(8,128)(2,1)S(1)}, bf16[512,512]{1,0:T(8,128)(2,1)}, u32[]{:S(2)}) copy-start(bf16[512,512]{1,0:T(8,128)(2,1)} %param.10) | copy-start | bytes 1572868
  395.5 127.0 %all-gather.20.cloned.1.call-start = ((), (), s32[]{:S(2)}) async-start(), calls=%async_computation.6 | async-start | bytes 4718592 | tf_op jit(solution)/shard_map/all_gather | solution.py:55
  440.5 3.4 copy-start.1
  440.5 8.5 %slice-start = ((s8[8388608]{0:T(1024)(128)(4,1)}), s8[4194304]{0:T(1024)(128)(4,1)S(1)}, s32[]{:S(2)}) async-start(s8[8388608]{0:T(1024)(128)(4,1)} %bitcast.194), calls=%async_computation.7 | async-start | bytes 8388608
  443.9 5.0 slice-start.1
  451.4 5.0 collective-permute-start.1
  476.6 66.7 %copy-start = (bf16[512,512]{1,0:T(8,128)(2,1)S(1)}, bf16[512,512]{1,0:T(8,128)(2,1)}, u32[]{:S(2)}) copy-start(bf16[512,512]{1,0:T(8,128)(2,1)} %fusion.33) | copy-start | bytes 1572868
Sparse Core Ops, SparseCore 0:
  9.0 49.5 all-gather.7
  60.4 86.2 all-gather.11
  148.6 87.4 all-gather.9
  237.8 87.4 all-gather.15
  326.8 46.8 all-gather.13
  395.7 44.7 all-gather.17
  476.7 45.7 all-gather.19
where the time goes:
time: 551 us
  waiting for transfers between devices  419 us (76%)
  blocking collectives  58.7 us (11%)
  matrix products  30.8 us (6%)
  other arithmetic  21.7 us (4%)
  between operations  13.8 us (3%)
  starting transfers between devices  7.2 us (1%)
    all_gather x2, waiting for transfers between devices, shards(): whole_mixed = lax.all_gather(mixed, 'tp', axis=1, tiled=True)  94.2 us
    all_gather x2, waiting for transfers between devices, shards(): gathered = lax.all_gather(stream, 'tp', axis=1, tiled=True)  93.7 us
    all_gather x1, waiting for transfers between devices, shards(): lax.all_gather(w_gate, 'sp', axis=1, tiled=True)  85.1 us
    all_gather x1, waiting for transfers between devices, shards(): lax.all_gather(w_value, 'sp', axis=1, tiled=True)  83.4 us
    all_gather x1, waiting for transfers between devices, shards(): lax.all_gather(w_out, 'sp', axis=1, tiled=True)  56.5 us
    psum x2, blocking collectives, shards(): total = lax.psum(jnp.sum(branch * branch, axis=-1), 'tp')  29.6 us
    psum x2, blocking collectives, shards(): lax.psum((jnp.sum(filtered, axis=-1), jnp.sum(filtered * filtered, axis=-...  29.1 us
    dot_general x2, matrix products, shards(): jnp.dot(whole_mixed, out_block, preferred_element_type=jnp.float32)  11.6 us
  transfers between devices with their start and end apart: 9, of which 9 were waited for; matrix products, arithmetic and copies ran while one was open for 4% of the time, Pallas kernels for 0%

commit v1 on v0

--- a/solution.py
+++ b/solution.py
@@ -21,7 +21,7 @@
     every_value, every_gate, every_out = (
         lax.all_gather(w_value, "sp", axis=1, tiled=True),
         lax.all_gather(w_gate, "sp", axis=1, tiled=True),
-        lax.all_gather(w_out, "sp", axis=1, tiled=True),
+        jnp.concatenate(lax.all_gather(w_out, "sp"), axis=1),
     )
     stream = tokens
     for layer_index in range(layer_count):

time: 551 us -> 551 us (level)
  waiting for transfers between devices: 419 us -> 413 us
  local copies, waits for them, and re-layouts: 0.46 us -> 6.22 us
    slice x0 -> x1, local copies, waits for them, and re-layouts: none -> 5.76 us  [shards(): out_block = every_out[layer_index]]
    all_gather x2, waiting for transfers between devices: 94.2 us -> 88.5 us  [shards(): whole_mixed = lax.all_gather(mixed, 'tp', axis=1, tiled=True)]
  transfers between devices with their start and end apart: 9 -> 9, of which waited for: 9 -> 9; matrix products, arithmetic and copies ran while one was open for 4% -> 5% of each run, Pallas kernels for 0% -> 0%
where the time goes in v1:
time: 551 us
  waiting for transfers between devices  413 us (75%)
  blocking collectives  58.7 us (11%)
  matrix products  30.9 us (6%)
  other arithmetic  21.6 us (4%)
  between operations  13.8 us (3%)
  starting transfers between devices  7.2 us (1%)
  local copies, waits for them, and re-layouts  6.22 us (1%)
    all_gather x2, waiting for transfers between devices, shards(): gathered = lax.all_gather(stream, 'tp', axis=1, tiled=True)  93.7 us
    all_gather x2, waiting for transfers between devices, shards(): whole_mixed = lax.all_gather(mixed, 'tp', axis=1, tiled=True)  88.5 us
    all_gather x1, waiting for transfers between devices, shards(): lax.all_gather(w_gate, 'sp', axis=1, tiled=True)  85.1 us
    all_gather x1, waiting for transfers between devices, shards(): lax.all_gather(w_value, 'sp', axis=1, tiled=True)  83.4 us
    all_gather x1, waiting for transfers between devices, shards(): lax.all_gather(w_out, 'sp')  56.5 us
    psum x2, blocking collectives, shards(): total = lax.psum(jnp.sum(branch * branch, axis=-1), 'tp')  29.6 us
    psum x2, blocking collectives, shards(): lax.psum((jnp.sum(filtered, axis=-1), jnp.sum(filtered * filtered, axis=-...  29 us
    dot_general x2, matrix products, shards(): jnp.dot(whole_mixed, out_block, preferred_element_type=jnp.float32)  11.7 us
  transfers between devices with their start and end apart: 9, of which 9 were waited for; matrix products, arithmetic and copies ran while one was open for 5% of the time, Pallas kernels for 0%

profile of v1, /device:TPU:0, one launch (start us, length us, event | category | flops | bytes accessed | tf_op | source)
XLA Modules:
  0.0 551.2 jit_solution(2187730576667447221)
XLA Ops:
  6.5 0.0 all-gather.9.cloned.1.call-start
  6.6 0.7 all-gather.9.cloned.1.call-update
  7.3 0.0 all-gather.13.cloned.1.call-start
  7.3 0.7 all-gather.13.cloned.1.call-update
  8.0 0.0 all-gather.11.cloned.1.call-start
  8.1 0.7 all-gather.11.cloned.1.call-update
  8.8 0.0 all-gather.21.cloned.1.call-start
  8.8 0.5 all-gather.21.cloned.1.call-update
  9.3 0.0 all-gather.15.cloned.1.call-start
  9.6 49.0 %all-gather.9.cloned.1.call-done = bf16[512,4096]{1,0:T(8,128)(2,1)} async-done(((bf16[512,512]{1,0:T(8,128)(2,1)}), bf16[512,4096]{1,0:T(8,128)(2,1)}) %all-gather.9.cloned.1.call-update) | async-done | bytes 4194320 | tf_op jit(solution)/shard_map/all_gather | solution.py:28
  58.6 3.1 fusion
  61.7 85.1 %all-gather.13.cloned.1.call-done = bf16[2,4096,512]{2,1,0:T(8,128)(2,1)} async-done(((bf16[2,1024,512]{2,1,0:T(8,128)(2,1)}), bf16[2,4096,512]{2,1,0:T(8,128)(2,1)}) %all-gather.13.cloned.1.call-update) | async-done | bytes 8388624 | tf_op jit(solution)/shard_map/all_gather | solution.py:23
  146.7 6.0 %fusion.19 = f32[512,512]{1,0:T(8,128)S(1)} fusion(bf16[2,4096,512]{2,1,0:T(8,128)(2,1)} %all-gather.13.cloned.1.call-done, bf16[512,4096]{1,0:T(8,128)(2,1)} %all-gather.9.cloned.1.call-done, f32[4096]{0:T(1024)S(1)} %bitcast.122, f32[512]{0:T(512)S(1)} %add_rsqrt_fusion.5), kind=kOutput, calls=%fused_computation.31 | convolution fusion | flops 2156658688 | bytes 9455616 | tf_op jit(solution)/shard_map/dot_general | solution.py:36
  152.7 83.4 %all-gather.11.cloned.1.call-done = bf16[2,4096,512]{2,1,0:T(8,128)(2,1)} async-done(((bf16[2,1024,512]{2,1,0:T(8,128)(2,1)}), bf16[2,4096,512]{2,1,0:T(8,128)(2,1)}) %all-gather.11.cloned.1.call-update) | async-done | bytes 8388624 | tf_op jit(solution)/shard_map/all_gather | solution.py:22
  236.1 5.8 %fusion.21 = bf16[512,512]{1,0:T(8,128)(2,1)S(1)} fusion(f32[512,512]{1,0:T(8,128)S(1)} %fusion.19, bf16[2,4096,512]{2,1,0:T(8,128)(2,1)} %all-gather.11.cloned.1.call-done, bf16[512,4096]{1,0:T(8,128)(2,1)} %all-gather.9.cloned.1.call-done, f32[4096]{0:T(1024)S(1)} %bitcast.123, f32[512]{0:T(512)S(1)} %add_rsqrt_fusion.5), kind=kOutput, calls=%fused_computation.33 | convolution fusion | flops 2156396544 | bytes 9979904 | tf_op jit(solution)/shard_map/dot_general | solution.py:35
  242.0 3.4 collective-permute-start
  245.4 1.6 collective-permute-done
  246.9 0.2 maximum_convert_fusion
  247.1 5.0 fusion.97
  252.1 15.3 %all-reduce.1 = (f32[512]{0:T(512)S(1)}, f32[512]{0:T(512)S(1)}) all-reduce(f32[512]{0:T(512)S(1)} %get-tuple-element.8, f32[512]{0:T(512)S(1)} %get-tuple-element.7), channel_id=1, replica_groups=mesh['sp'=4,'tp'=8] {'tp'}, use_global_device_ids=true, to_apply=%region_4.0 | all-reduce | flops 1024 | bytes 8192 | tf_op jit(solution)/shard_map/psum | solution.py:46
  267.4 1.2 multiply_convert_fusion.1
  268.7 0.0 all-gather.15.cloned.1.call-update
  268.7 0.0 all-gather.17.cloned.1.call-start
  268.8 56.5 %all-gather.21.cloned.1.call-done = bf16[8,1024,512]{2,1,0:T(8,128)(2,1)} async-done(((bf16[2,1024,512]{2,1,0:T(8,128)(2,1)}), bf16[8,1024,512]{2,1,0:T(8,128)(2,1)}) %all-gather.21.cloned.1.call-update) | async-done | bytes 8388624 | tf_op jit(solution)/shard_map/all_gather | solution.py:24
  325.3 5.8 %fusion.100 = (bf16[1,4,1024,512]{3,2,0,1:T(8,128)(2,1)}, bf16[1,4,1024,512]{3,2,0,1:T(8,128)(2,1)}) fusion(bf16[2,4,1024,512]{3,2,0,1:T(8,128)(2,1)} %bitcast.117), kind=kLoop, calls=%fused_computation.184 | loop fusion | bytes 16777216 | tf_op jit(solution)/shard_map/slice | solution.py:34
  331.1 42.6 %all-gather.15.cloned.1.call-done = bf16[512,4096]{1,0:T(8,128)(2,1)} async-done(((bf16[512,512]{1,0:T(8,128)(2,1)}), bf16[512,4096]{1,0:T(8,128)(2,1)}) %all-gather.15.cloned.1.call-update) | async-done | bytes 4194320 | tf_op jit(solution)/shard_map/all_gather | solution.py:55
  373.7 5.8 %convolution_convert_fusion.1 = bf16[512,512]{1,0:T(8,128)(2,1)S(1)} fusion(bf16[512,4096]{1,0:T(8,128)(2,1)} %all-gather.15.cloned.1.call-done, bf16[4096,512]{1,0:T(8,128)(2,1)} %bitcast.119), kind=kOutput, calls=%fused_computation.35 | convolution fusion | flops 2147745792 | bytes 8912896 | tf_op jit(solution)/shard_map/dot_general | solution.py:56
  379.5 0.2 fusion.26
  379.7 14.8 %psum.44 = f32[512]{0:T(512)S(1)} all-reduce(f32[512]{0:T(512)S(1)} %fusion.26), channel_id=1, replica_groups=mesh['sp'=4,'tp'=8] {'tp'}, use_global_device_ids=true, to_apply=%region_6.7 | all-reduce | flops 512 | bytes 4096 | tf_op jit(solution)/shard_map/psum | solution.py:60
  394.5 1.1 fusion.29
  395.6 0.0 all-gather.17.cloned.1.call-update
  395.6 0.2 all-gather.19.cloned.1.call-start
  395.8 44.7 %all-gather.17.cloned.1.call-done = bf16[512,4096]{1,0:T(8,128)(2,1)} async-done(((bf16[512,512]{1,0:T(8,128)(2,1)}), bf16[512,4096]{1,0:T(8,128)(2,1)}) %all-gather.17.cloned.1.call-update) | async-done | bytes 4194320 | tf_op jit(solution)/shard_map/all_gather | solution.py:28
  440.5 3.2 fusion.3
  443.8 0.2 copy-done.1
  444.0 5.0 fusion.17
  449.0 2.4 fusion.20
  451.4 3.4 collective-permute-start.1
  454.9 1.5 collective-permute-done.1
  456.4 0.2 maximum_convert_fusion.1
  456.5 5.0 fusion.96
  461.5 13.7 %all-reduce = (f32[512]{0:T(512)S(1)}, f32[512]{0:T(512)S(1)}) all-reduce(f32[512]{0:T(512)S(1)} %get-tuple-element.6, f32[512]{0:T(512)S(1)} %get-tuple-element.5), channel_id=1, replica_groups=mesh['sp'=4,'tp'=8] {'tp'}, use_global_device_ids=true, to_apply=%region_11.12 | all-reduce | flops 1024 | bytes 8192 | tf_op jit(solution)/shard_map/psum | solution.py:46
  475.3 1.2 multiply_convert_fusion
  476.5 45.9 %all-gather.19.cloned.1.call-done = bf16[512,4096]{1,0:T(8,128)(2,1)} async-done(((bf16[512,512]{1,0:T(8,128)(2,1)}), bf16[512,4096]{1,0:T(8,128)(2,1)}) %all-gather.19.cloned.1.call-update) | async-done | bytes 4194320 | tf_op jit(solution)/shard_map/all_gather | solution.py:55
  522.4 5.8 %convolution_convert_fusion = bf16[512,512]{1,0:T(8,128)(2,1)S(1)} fusion(bf16[512,4096]{1,0:T(8,128)(2,1)} %all-gather.19.cloned.1.call-done, bf16[4096,512]{1,0:T(8,128)(2,1)} %bitcast.118), kind=kOutput, calls=%fused_computation.34 | convolution fusion | flops 2147745792 | bytes 8912896 | tf_op jit(solution)/shard_map/dot_general | solution.py:56
  528.3 0.2 fusion.30
  528.4 14.8 %psum.47 = f32[512]{0:T(512)S(1)} all-reduce(f32[512]{0:T(512)S(1)} %fusion.30), channel_id=1, replica_groups=mesh['sp'=4,'tp'=8] {'tp'}, use_global_device_ids=true, to_apply=%region_13.14 | all-reduce | flops 512 | bytes 4096 | tf_op jit(solution)/shard_map/psum | solution.py:60
  543.3 1.1 fusion.33
  (40 shorter events, 0.3 us)
Async XLA Ops:
  6.5 2.8 copy-start.5
  6.5 2.9 copy-start.6
  6.5 2.9 copy-start.3
  6.5 3.0 copy-start.4
  6.5 52.0 %all-gather.9.cloned.1.call-start = ((), (), s32[]{:S(2)}) async-start(), calls=%async_computation | async-start | bytes 4718592 | tf_op jit(solution)/shard_map/all_gather | solution.py:28
  7.3 139.5 %all-gather.13.cloned.1.call-start = ((), (), s32[]{:S(2)}) async-start(), calls=%async_computation.2 | async-start | bytes 10485760 | tf_op jit(solution)/shard_map/all_gather | solution.py:23
  8.0 228.1 %all-gather.11.cloned.1.call-start = ((), (), s32[]{:S(2)}) async-start(), calls=%async_computation.1 | async-start | bytes 10485760 | tf_op jit(solution)/shard_map/all_gather | solution.py:22
  8.8 316.6 %all-gather.21.cloned.1.call-start = ((), (), s32[]{:S(2)}) async-start(), calls=%async_computation.6 | async-start | bytes 10485760 | tf_op jit(solution)/shard_map/all_gather | solution.py:24
  9.3 364.3 %all-gather.15.cloned.1.call-start = ((), (), s32[]{:S(2)}) async-start(), calls=%async_computation.3 | async-start | bytes 4718592 | tf_op jit(solution)/shard_map/all_gather | solution.py:55
  152.7 92.6 %copy-start.7 = (f32[2,512]{1,0:T(2,128)S(1)}, f32[2,512]{1,0:T(2,128)}, u32[]{:S(2)}) copy-start(f32[2,512]{1,0:T(2,128)} %param.17) | copy-start | bytes 12292
  242.0 5.0 collective-permute-start
  247.1 21.6 %copy-start.8 = (f32[2,512]{1,0:T(2,128)S(1)}, f32[2,512]{1,0:T(2,128)}, u32[]{:S(2)}) copy-start(f32[2,512]{1,0:T(2,128)} %param.19) | copy-start | bytes 12292
  268.7 171.8 %all-gather.17.cloned.1.call-start = ((), (), s32[]{:S(2)}) async-start(), calls=%async_computation.4 | async-start | bytes 4718592 | tf_op jit(solution)/shard_map/all_gather | solution.py:28
  373.7 20.8 %copy-start.2 = (bf16[512,512]{1,0:T(8,128)(2,1)S(1)}, bf16[512,512]{1,0:T(8,128)(2,1)}, u32[]{:S(2)}) copy-start(bf16[512,512]{1,0:T(8,128)(2,1)} %param.10) | copy-start | bytes 1572868
  395.6 126.9 %all-gather.19.cloned.1.call-start = ((), (), s32[]{:S(2)}) async-start(), calls=%async_computation.5 | async-start | bytes 4718592 | tf_op jit(solution)/shard_map/all_gather | solution.py:55
  440.5 3.4 copy-start.1
  440.5 8.5 %slice-start = ((s8[8388608]{0:T(1024)(128)(4,1)}), s8[4194304]{0:T(1024)(128)(4,1)S(1)}, s32[]{:S(2)}) async-start(s8[8388608]{0:T(1024)(128)(4,1)} %bitcast.194), calls=%async_computation.7 | async-start | bytes 8388608
  444.0 5.0 slice-start.1
  451.4 5.0 collective-permute-start.1
  522.4 20.8 %copy-start = (bf16[512,512]{1,0:T(8,128)(2,1)S(1)}, bf16[512,512]{1,0:T(8,128)(2,1)}, u32[]{:S(2)}) copy-start(bf16[512,512]{1,0:T(8,128)(2,1)} %fusion.29) | copy-start | bytes 1572868
Sparse Core Ops, SparseCore 0:
  9.0 49.5 all-gather.8
  60.4 86.2 all-gather.12
  148.6 87.4 all-gather.10
  237.8 87.4 all-gather.20
  326.8 46.8 all-gather.14
  395.7 44.7 all-gather.16
  476.7 45.7 all-gather.18
